TPU v7x, 32 devices: a whole 2x2x4 slice. The times are simulated.
32 devices in a mesh: rep: 2 (over x), fs: 4 (over z), tp: 4 (over y, core).
Axes of the slice: x: 2, y: 2, z: 4, core: 2. Of those that a mesh axis runs over, the one named last changes fastest.
Arguments:
- tokens: bfloat16 [8192, 2048], P(('rep', 'fs'), 'tp'), may hold values from -6 to 6
- mix_gain: float32 [2048], replicated, may hold values from 0.1 to 1.9
- query_weight: bfloat16 [2048, 512], P('fs', 'tp'), may hold values from -0.125 to 0.125
- key_weight: bfloat16 [2048, 512], P('fs', 'tp'), may hold values from -0.125 to 0.125
- value_weight: bfloat16 [2048, 1024], P('fs', 'tp'), may hold values from -0.125 to 0.125
- gate_weight: bfloat16 [2048, 1024], P('fs', 'tp'), may hold values from -0.125 to 0.125
- out_weight: bfloat16 [1024, 2048], P('tp', 'fs'), may hold values from -0.1875 to 0.1875
- head_gain: float32 [8, 128], P('tp'), may hold values from 0.1 to 1.9
- ffn_gain: float32 [2048], replicated, may hold values from 0.1 to 1.9
- ffn_gate: bfloat16 [2048, 5632], P('fs', 'tp'), may hold values from -0.125 to 0.125
- ffn_up: bfloat16 [2048, 5632], P('fs', 'tp'), may hold values from -0.125 to 0.125
- ffn_down: bfloat16 [5632, 2048], P('tp', 'fs'), may hold values from -0.078125 to 0.078125
Outputs:
- layer_out: bfloat16 [8192, 2048], P(('rep', 'fs'), 'tp')
All inputs are finite; a program needn't handle non-finite values.
Results may differ from a plain program's by a relative error of at most 0.03.
Values may be sent and summed in bfloat16 or wider, within the bound.
A program may use at most 128 MiB of HBM per device.

v0:
```python
import jax
import jax.numpy as jnp
from jax import lax
from jax.sharding import PartitionSpec as P

HEADS = 8
DK = 64
DV = 128
BLOCK = 64
SEQ = 256
epsilon = 1e-06
rope_base = 10000.0


def norm_rows(values, gain_row):
    floats = values.astype(jnp.float32)
    scaled = floats * lax.rsqrt(jnp.mean(floats * floats, axis=-1, keepdims=True) + epsilon)
    return (scaled * gain_row).astype(jnp.bfloat16)


def rotate(values, positions):
    half_dim = values.shape[-1] // 2
    frequency = rope_base ** (-jnp.linspace(0.0, 1.0, half_dim, dtype=jnp.float32))
    angles = positions.astype(jnp.float32)[:, None] * frequency[None, :]
    cosine = jnp.cos(angles)[:, None, :]
    sine_part = jnp.sin(angles)[:, None, :]
    paired = values.reshape(values.shape[:-1] + (half_dim, 2))
    leading = paired[..., 0]
    trailing = paired[..., 1]
    turned = jnp.stack(
        [leading * cosine - trailing * sine_part, leading * sine_part + trailing * cosine], axis=-1
    )
    return turned.reshape(values.shape)


def log_decay(head_index, total_heads):
    return jnp.log1p(-jnp.exp2(-5.0 - 4.0 * head_index.astype(jnp.float32) / (total_heads - 1)))


def retention(queries, key_rows, value_rows, decay_rates):
    highest = lax.Precision.HIGHEST
    row_count, head_count = (queries.shape[0], queries.shape[1])
    seq_count = row_count // SEQ
    block_count = SEQ // BLOCK

    def to_blocks(values):
        shaped = values.reshape((seq_count, block_count, BLOCK) + values.shape[1:])
        return jnp.moveaxis(shaped, 1, 0)

    inside = jnp.arange(BLOCK, dtype=jnp.int32)
    gap = (inside[:, None] - inside[None, :]).astype(jnp.float32)
    within_mask = jnp.where(
        gap[None] >= 0.0, jnp.exp(jnp.maximum(gap, 0.0)[None] * decay_rates[:, None, None]), 0.0
    )
    query_scale = jnp.exp((inside + 1).astype(jnp.float32)[:, None] * decay_rates[None, :])
    key_scale = jnp.exp((BLOCK - 1 - inside).astype(jnp.float32)[:, None] * decay_rates[None, :])
    block_decay = jnp.exp(BLOCK * decay_rates)

    def advance(state, inputs):
        query_blk, key_blk, value_blk = inputs
        scores = (
            jnp.einsum("sihd,sjhd->shij", query_blk, key_blk, precision=highest) * within_mask[None]
        )
        local_part = jnp.einsum("shij,sjhv->sihv", scores, value_blk, precision=highest)
        carried = jnp.einsum(
            "sihd,shdv->sihv", query_blk * query_scale[None, :, :, None], state, precision=highest
        )
        update = jnp.einsum(
            "sjhd,sjhv->shdv", key_blk * key_scale[None, :, :, None], value_blk, precision=highest
        )
        return (block_decay[None, :, None, None] * state + update, local_part + carried)

    state_zero = jnp.zeros((seq_count, head_count, DK, DV), jnp.float32)
    _, outputs = lax.scan(
        advance, state_zero, (to_blocks(queries), to_blocks(key_rows), to_blocks(value_rows))
    )
    return jnp.moveaxis(outputs, 0, 1).reshape(row_count, head_count, DV)


def per_device(
    tokens,
    mix_gain,
    query_weight,
    key_weight,
    value_weight,
    gate_weight,
    out_weight,
    head_gain,
    ffn_gain,
    ffn_gate,
    ffn_up,
    ffn_down,
):
    whole_rows = lax.all_gather(tokens, "tp", axis=1, tiled=True)
    row_count = whole_rows.shape[0]
    normed = norm_rows(whole_rows, mix_gain)
    pieces = (
        lax.all_gather(query_weight, "fs", axis=0, tiled=True),
        lax.all_gather(key_weight, "fs", axis=0, tiled=True),
        lax.all_gather(value_weight, "fs", axis=0, tiled=True),
        lax.all_gather(gate_weight, "fs", axis=0, tiled=True),
    )
    query_acc, key_acc, value_acc, gate_acc = tuple(
        (
            jnp.dot(normed, weight_piece, preferred_element_type=jnp.float32)
            for weight_piece in pieces
        )
    )
    heads_here = query_weight.shape[1] // DK
    positions = jnp.arange(row_count, dtype=jnp.int32) % SEQ
    queries = rotate(
        query_acc.astype(jnp.bfloat16).astype(jnp.float32).reshape(row_count, heads_here, DK),
        positions,
    )
    key_rows = rotate(
        key_acc.astype(jnp.bfloat16).astype(jnp.float32).reshape(row_count, heads_here, DK),
        positions,
    ) * DK ** (-0.5)
    value_rows = (
        value_acc.astype(jnp.bfloat16).astype(jnp.float32).reshape(row_count, heads_here, DV)
    )
    gate_rows = gate_acc.astype(jnp.bfloat16).astype(jnp.float32)
    first_head = lax.axis_index("tp") * heads_here
    decay_rates = log_decay(first_head + jnp.arange(heads_here, dtype=jnp.int32), HEADS)
    retained = retention(queries, key_rows, value_rows, decay_rates)
    center = jnp.mean(retained, axis=-1, keepdims=True)
    spread = jnp.mean(jnp.square(retained - center), axis=-1, keepdims=True)
    grouped = (retained - center) * lax.rsqrt(spread + epsilon) * head_gain[None]
    mixed = (grouped.reshape(row_count, heads_here * DV) * jax.nn.silu(gate_rows)).astype(
        jnp.bfloat16
    )
    mixer_terms = jnp.dot(
        mixed,
        lax.all_gather(out_weight, "fs", axis=1, tiled=True),
        preferred_element_type=jnp.float32,
    )
    mixer_share = lax.psum_scatter(
        mixer_terms.astype(jnp.bfloat16), "tp", scatter_dimension=1, tiled=True
    ).astype(jnp.float32)
    resid_shard = (tokens.astype(jnp.float32) + mixer_share).astype(jnp.bfloat16)
    resid_whole = lax.all_gather(resid_shard, "tp", axis=1, tiled=True)
    normed_ffn = norm_rows(resid_whole, ffn_gain)

    def add_rows(weight_piece):
        return jnp.dot(normed_ffn, weight_piece, preferred_element_type=jnp.float32)

    gate_hidden = add_rows(lax.all_gather(ffn_gate, "fs", axis=0, tiled=True))
    up_hidden = add_rows(lax.all_gather(ffn_up, "fs", axis=0, tiled=True))
    hidden = (jax.nn.silu(gate_hidden) * up_hidden).astype(jnp.bfloat16)
    ffn_terms = jnp.dot(
        hidden,
        lax.all_gather(ffn_down, "fs", axis=1, tiled=True),
        preferred_element_type=jnp.float32,
    )
    ffn_share = lax.psum_scatter(
        ffn_terms.astype(jnp.bfloat16), "tp", scatter_dimension=1, tiled=True
    ).astype(jnp.float32)
    return (resid_shard.astype(jnp.float32) + ffn_share).astype(jnp.bfloat16)


def solution(mesh):
    return jax.shard_map(
        per_device,
        mesh=mesh,
        in_specs=(
            P(("rep", "fs"), "tp"),
            P(),
            P("fs", "tp"),
            P("fs", "tp"),
            P("fs", "tp"),
            P("fs", "tp"),
            P("tp", "fs"),
            P("tp", None),
            P(),
            P("fs", "tp"),
            P("fs", "tp"),
            P("tp", "fs"),
        ),
        out_specs=P(("rep", "fs"), "tp"),
        check_vma=False,
    )
```

profile of v0, /device:TPU:0, one launch (start us, length us, event | category | flops | bytes accessed | tf_op | source)
XLA Modules:
  0.0 622.1 jit_solution(10062320432352257111)
XLA Ops:
  6.5 0.7 all-gather.9.cloned.1.call-update
  7.3 0.7 all-gather.11.cloned.1.call-update
  8.1 0.7 all-gather.13.cloned.1.call-update
  8.8 0.5 all-gather.15.cloned.1.call-update
  9.5 17.6 %all_gather.31 = bf16[2048,128]{1,0:T(8,128)(2,1)S(1)} all-gather(bf16[512,128]{1,0:T(8,128)(2,1)} %param.19), channel_id=1, replica_groups=mesh['rep'=2,'fs'=4,'tp'=4] {'fs'}, dimensions={0}, use_global_device_ids=true | all-gather | bytes 655360 | tf_op jit(solution)/shard_map/all_gather | solution.py:99
  27.0 16.6 %all_gather.33 = bf16[2048,128]{1,0:T(8,128)(2,1)S(1)} all-gather(bf16[512,128]{1,0:T(8,128)(2,1)} %param.18), channel_id=1, replica_groups=mesh['rep'=2,'fs'=4,'tp'=4] {'fs'}, dimensions={0}, use_global_device_ids=true | all-gather | bytes 655360 | tf_op jit(solution)/shard_map/all_gather | solution.py:98
  43.7 1.3 multiply_cosine_fusion
  45.0 1.2 all-gather.9.cloned.1.call-done
  46.1 3.2 fusion.25
  49.6 1.0 fusion.27
  50.6 1.9 copy-done
  52.5 1.5 fusion.36
  54.1 0.3 reshape.185
  54.4 3.9 fusion.35
  58.5 2.1 multiply_subtract_fusion
  60.6 1.0 maximum_multiply_fusion
  61.6 1.8 mul.286
  63.4 1.9 reshape_reshape.24
  65.3 10.4 %all-gather.11.cloned.1.call-done = bf16[2048,256]{1,0:T(8,128)(2,1)} async-done(((bf16[512,256]{1,0:T(8,128)(2,1)}), bf16[2048,256]{1,0:T(8,128)(2,1)}) %all-gather.11.cloned.1.call-update) | async-done | bytes 1048592 | tf_op jit(solution)/shard_map/all_gather | solution.py:100
  75.7 3.7 fusion.31
  79.4 0.5 reshape.187
  80.1 19.0 %while.15 = (s32[]{:T(128)}, f32[4,2,64,128]{3,2,1,0:T(8,128)S(1)}, f32[4,4,64,2,128]{4,2,3,1,0:T(8,128)S(1)}, f32[4,4,64,2,64]{2,0,1,4,3:T(4,128)}, f32[4,4,64,...) while((s32[]{:T(128)}, f32[4,2,64,128]{3,2,1,0:T(8,128)S(1)}, ...), condition=%wide.region_2.4_spmd.clone.clone.clone, body=%wide.region_1.3_spmd.clone.clone.clone.sunk | while | flops 176603408 | bytes 4415676 | solution.py:74
  80.3 2.1 constant_dynamic-slice_fusion.3
  82.8 0.5 convolution_multiply_fusion.2
  83.3 0.4 convolution_bitcast_fusion.3
  83.8 0.4 fusion.93
  84.3 0.7 convolution_add_fusion.2
  85.0 2.1 constant_dynamic-slice_fusion.3
  87.5 0.5 convolution_multiply_fusion.2
  88.0 0.4 convolution_bitcast_fusion.3
  88.5 0.4 fusion.93
  89.0 0.7 convolution_add_fusion.2
  89.7 2.1 constant_dynamic-slice_fusion.3
  92.2 0.5 convolution_multiply_fusion.2
  92.7 0.4 convolution_bitcast_fusion.3
  93.2 0.4 fusion.93
  93.7 0.7 convolution_add_fusion.2
  94.4 2.1 constant_dynamic-slice_fusion.3
  96.9 0.5 convolution_multiply_fusion.2
  97.4 0.4 convolution_bitcast_fusion.3
  97.9 0.4 fusion.93
  98.4 0.7 convolution_add_fusion.2
  99.1 0.4 bitcast_reduce_fusion
  99.7 0.7 multiply_reduce_fusion
  100.7 1.8 copy.35
  102.5 2.2 all-gather.13.cloned.1.call-done
  104.7 28.8 %all-gather.15.cloned.1.call-done = bf16[256,2048]{1,0:T(8,128)(2,1)} async-done(((bf16[256,512]{1,0:T(8,128)(2,1)}), bf16[256,2048]{1,0:T(8,128)(2,1)}) %all-gather.15.cloned.1.call-update) | async-done | bytes 1048592 | tf_op jit(solution)/shard_map/all_gather | solution.py:134
  133.5 1.2 mul.299
  134.7 2.0 sub.86
  136.8 9.9 %convolution_convert_fusion.1 = bf16[1024,2048]{1,0:T(8,128)(2,1)} fusion(bf16[256,2048]{1,0:T(8,128)(2,1)} %all-gather.15.cloned.1.call-done, bf16[1024,2048]{1,0:T(8,128)(2,1)} %copy-done, bf16[2048,256]{1,0:T(8,128)(2,1)} %all-gather.13.cloned.1.call-done, f32[128,8,2,128]{3,2,1,0:T(2,128)S(1)} %bitcast.114, f32[128,8,2,128]{3,2,1,0:T(2,128)} %bitcast.115, ...), kind=kOutput, calls=%fused_computation.45 | convolution fusion | flops 2152464384 | bytes 13632512 | tf_op jit(solution)/shard_map/dot_general | solution.py:132
  146.8 43.9 %reduce-scatter.3.cloned.1.call-done = bf16[1024,512]{1,0:T(8,128)(2,1)} async-done(((bf16[1024,2048]{1,0:T(8,128)(2,1)}), bf16[1024,512]{1,0:T(8,128)(2,1)}) %reduce-scatter.3.cloned.1.call-update) | async-done | bytes 1048592 | tf_op jit(solution)/shard_map/reduce_scatter | solution.py:137
  190.6 2.5 add_convert_fusion.1
  193.2 0.7 all-gather.19.cloned.1.call-update
  193.9 0.7 all-gather.21.cloned.1.call-update
  194.7 0.7 all-gather.23.cloned.1.call-update
  195.4 32.3 %all-gather.17.cloned.1.call-done = bf16[1024,2048]{1,0:T(8,128)(2,1)} async-done(((bf16[1024,512]{1,0:T(8,128)(2,1)}), bf16[1024,2048]{1,0:T(8,128)(2,1)}) %all-gather.17.cloned.1.call-update) | async-done | bytes 4194320 | tf_op jit(solution)/shard_map/all_gather | solution.py:141
  227.7 3.1 fusion.28
  230.8 105.2 %all-gather.19.cloned.1.call-done = bf16[2048,1408]{1,0:T(8,128)(2,1)} async-done(((bf16[512,1408]{1,0:T(8,128)(2,1)}), bf16[2048,1408]{1,0:T(8,128)(2,1)}) %all-gather.19.cloned.1.call-update) | async-done | bytes 5767184 | tf_op jit(solution)/shard_map/all_gather | solution.py:147
  336.0 11.9 %fusion.33 = f32[1024,1408]{1,0:T(8,128)} fusion(bf16[2048,1408]{1,0:T(8,128)(2,1)} %all-gather.19.cloned.1.call-done, bf16[1024,2048]{1,0:T(8,128)(2,1)} %all-gather.17.cloned.1.call-done, f32[2048]{0:T(1024)S(1)} %copy-done.5, f32[1024]{0:T(1024)S(1)} %add_rsqrt_fusion), kind=kOutput, calls=%fused_computation.53 | convolution fusion | flops 5913968640 | bytes 15740928 | tf_op jit(solution)/shard_map/dot_general | solution.py:145
  347.9 94.7 %all-gather.21.cloned.1.call-done = bf16[2048,1408]{1,0:T(8,128)(2,1)} async-done(((bf16[512,1408]{1,0:T(8,128)(2,1)}), bf16[2048,1408]{1,0:T(8,128)(2,1)}) %all-gather.21.cloned.1.call-update) | async-done | bytes 5767184 | tf_op jit(solution)/shard_map/all_gather | solution.py:148
  442.6 106.5 %all-gather.23.cloned.1.call-done = bf16[1408,2048]{1,0:T(8,128)(2,1)} async-done(((bf16[1408,512]{1,0:T(8,128)(2,1)}), bf16[1408,2048]{1,0:T(8,128)(2,1)}) %all-gather.23.cloned.1.call-update) | async-done | bytes 5767184 | tf_op jit(solution)/shard_map/all_gather | solution.py:152
  549.1 20.9 %convolution_convert_fusion = bf16[1024,2048]{1,0:T(8,128)(2,1)} fusion(bf16[1408,2048]{1,0:T(8,128)(2,1)} %all-gather.23.cloned.1.call-done, f32[1024,1408]{1,0:T(8,128)} %fusion.33, bf16[2048,1408]{1,0:T(8,128)(2,1)} %all-gather.21.cloned.1.call-done, bf16[1024,2048]{1,0:T(8,128)(2,1)} %all-gather.17.cloned.1.call-done, f32[2048]{0:T(1024)S(1)} %copy-done.5, ...), kind=kOutput, calls=%fused_computation.44 | convolution fusion | flops 11830296576 | bytes 25702400 | tf_op jit(solution)/shard_map/dot_general | solution.py:150
  570.0 42.8 %reduce-scatter.5.cloned.1.call-done = bf16[1024,512]{1,0:T(8,128)(2,1)} async-done(((bf16[1024,2048]{1,0:T(8,128)(2,1)}), bf16[1024,512]{1,0:T(8,128)(2,1)}) %reduce-scatter.5.cloned.1.call-update) | async-done | bytes 1048592 | tf_op jit(solution)/shard_map/reduce_scatter | solution.py:155
  612.8 2.5 add_convert_fusion
  (64 shorter events, 3.6 us)
Async XLA Ops:
  6.5 42.8 %copy-start.4 = (f32[2048]{0:T(1024)S(1)}, f32[2048]{0:T(1024)}, u32[]{:S(2)}) copy-start(f32[2048]{0:T(1024)} %param.17) | copy-start | bytes 24580
  6.5 39.6 %all-gather.9.cloned.1.call-start = ((), (), s32[]{:S(2)}) async-start(), calls=%async_computation.2 | async-start | bytes 5242880 | tf_op jit(solution)/shard_map/all_gather | solution.py:94
  7.3 68.4 %all-gather.11.cloned.1.call-start = ((), (), s32[]{:S(2)}) async-start(), calls=%async_computation.3 | async-start | bytes 1310720 | tf_op jit(solution)/shard_map/all_gather | solution.py:100
  8.0 96.7 %all-gather.13.cloned.1.call-start = ((), (), s32[]{:S(2)}) async-start(), calls=%async_computation.4 | async-start | bytes 1310720 | tf_op jit(solution)/shard_map/all_gather | solution.py:101
  8.7 124.8 %all-gather.15.cloned.1.call-start = ((), (), s32[]{:S(2)}) async-start(), calls=%async_computation.5 | async-start | bytes 1310720 | tf_op jit(solution)/shard_map/all_gather | solution.py:134
  9.3 181.3 %reduce-scatter.3.cloned.1.call-start = ((), (), s32[]{:S(2)}) async-start(), calls=%async_computation.6 | async-start | bytes 5242880 | tf_op jit(solution)/shard_map/reduce_scatter | solution.py:137
  46.1 3.4 copy-start.1
  50.6 1.9 copy-start
  99.1 37.7 %copy-start.6 = (f32[2,128]{1,0:T(2,128)S(1)}, f32[2,128]{1,0:T(2,128)}, u32[]{:S(2)}) copy-start(f32[2,128]{1,0:T(2,128)} %param.23) | copy-start | bytes 3076
  136.8 53.9 %copy-start.3 = (bf16[1024,512]{1,0:T(8,128)(2,1)S(1)}, bf16[1024,512]{1,0:T(8,128)(2,1)}, u32[]{:S(2)}) copy-start(bf16[1024,512]{1,0:T(8,128)(2,1)} %param.16) | copy-start | bytes 3145732
  146.7 189.3 %copy-start.5 = (f32[2048]{0:T(1024)S(1)}, f32[2048]{0:T(1024)}, u32[]{:S(2)}) copy-start(f32[2048]{0:T(1024)} %param.24) | copy-start | bytes 24580
  146.7 81.0 %all-gather.17.cloned.1.call-start = ((), (), s32[]{:S(2)}) async-start(), calls=%async_computation.7 | async-start | bytes 5242880 | tf_op jit(solution)/shard_map/all_gather | solution.py:141
  193.1 142.9 %all-gather.19.cloned.1.call-start = ((), (), s32[]{:S(2)}) async-start(), calls=%async_computation.8 | async-start | bytes 7208960 | tf_op jit(solution)/shard_map/all_gather | solution.py:147
  193.9 248.7 %all-gather.21.cloned.1.call-start = ((), (), s32[]{:S(2)}) async-start(), calls=%async_computation.9 | async-start | bytes 7208960 | tf_op jit(solution)/shard_map/all_gather | solution.py:148
  194.6 354.5 %all-gather.23.cloned.1.call-start = ((), (), s32[]{:S(2)}) async-start(), calls=%async_computation.10 | async-start | bytes 7208960 | tf_op jit(solution)/shard_map/all_gather | solution.py:152
  195.4 417.5 %reduce-scatter.5.cloned.1.call-start = ((), (), s32[]{:S(2)}) async-start(), calls=%async_computation.11 | async-start | bytes 5242880 | tf_op jit(solution)/shard_map/reduce_scatter | solution.py:155
  347.9 264.9 %copy-start.2 = (bf16[1024,512]{1,0:T(8,128)(2,1)S(1)}, bf16[1024,512]{1,0:T(8,128)(2,1)}, u32[]{:S(2)}) copy-start(bf16[1024,512]{1,0:T(8,128)(2,1)} %add_convert_fusion.1) | copy-start | bytes 3145732
Sparse Core Ops, SparseCore 0:
  8.9 37.1 all-gather.8
  47.7 27.9 all-gather.10
  77.3 27.3 all-gather.12
  106.1 27.3 all-gather.14
  146.8 43.7 reduce-scatter.2
  193.2 34.4 all-gather.16
  229.3 106.6 all-gather.18
  337.6 104.9 all-gather.20
  444.1 104.9 all-gather.22
  570.1 42.6 reduce-scatter.4
where the time goes:
time: 623 us; the launch traced here: 622 us
  waiting for transfers between devices  473 us (76%)
  matrix products  60 us (10%)
  blocking collectives  34.1 us (5%)
  local copies, waits for them, and re-layouts  22.2 us (4%)
  other arithmetic  18.5 us (3%)
  between operations  13.7 us (2%)
    all_gather x1, waiting for transfers between devices, per_device(): lax.all_gather(ffn_down, 'fs', axis=1, tiled=True)  107 us
    all_gather x1, waiting for transfers between devices, per_device(): gate_hidden = add_rows(lax.all_gather(ffn_gate, 'fs', axis=0, tiled=True))  105 us
    all_gather x1, waiting for transfers between devices, per_device(): up_hidden = add_rows(lax.all_gather(ffn_up, 'fs', axis=0, tiled=True))  94.7 us
    reduce_scatter x1, waiting for transfers between devices, per_device(): lax.psum_scatter(mixer_terms.astype(jnp.bfloat16), 'tp', scatter_dimensio...  43.9 us
    reduce_scatter x1, waiting for transfers between devices, per_device(): lax.psum_scatter(ffn_terms.astype(jnp.bfloat16), 'tp', scatter_dimension=...  42.8 us
    all_gather x1, waiting for transfers between devices, per_device(): resid_whole = lax.all_gather(resid_shard, 'tp', axis=1, tiled=True)  32.3 us
    all_gather x1, waiting for transfers between devices, per_device(): lax.all_gather(out_weight, 'fs', axis=1, tiled=True)  28.8 us
    dot_general x1, matrix products, per_device(): jnp.dot(hidden, lax.all_gather(ffn_down, 'fs', axis=1, tiled=True), prefe...  20.9 us
  transfers between devices with their start and end apart: 10, of which 10 were waited for; matrix products, arithmetic and copies ran while one was open for 10% of the time, Pallas kernels for 0%

commit v1 on v0

--- a/solution.py
+++ b/solution.py
@@ -145,7 +145,11 @@
         return jnp.dot(normed_ffn, weight_piece, preferred_element_type=jnp.float32)
 
     gate_hidden = add_rows(lax.all_gather(ffn_gate, "fs", axis=0, tiled=True))
-    up_hidden = add_rows(lax.all_gather(ffn_up, "fs", axis=0, tiled=True))
+    up_hidden = add_rows(
+        jnp.concatenate(
+            lax.all_to_all(jnp.stack([ffn_up] * lax.axis_size("fs")), "fs", 0, 0), axis=0
+        )
+    )
     hidden = (jax.nn.silu(gate_hidden) * up_hidden).astype(jnp.bfloat16)
     ffn_terms = jnp.dot(
         hidden,

time: 623 us -> 602 us (0.966)
  waiting for transfers between devices: 473 us -> 444 us
    all_gather x1 -> x0, waiting for transfers between devices: 94.7 us -> none  [per_device(): up_hidden = add_rows(lax.all_gather(ffn_up, 'fs', axis=0, tiled=True))]
    all_gather x1, waiting for transfers between devices: 105 us -> 182 us  [per_device(): gate_hidden = add_rows(lax.all_gather(ffn_gate, 'fs', axis=0, tiled=True))]
    all_gather x1, waiting for transfers between devices: 32.3 us -> 24.7 us  [per_device(): resid_whole = lax.all_gather(resid_shard, 'tp', axis=1, tiled=True)]
  transfers between devices with their start and end apart: 10 -> 10, of which waited for: 10 -> 9; matrix products, arithmetic and copies ran while one was open for 10% -> 10% of each run, Pallas kernels for 0% -> 0%
where the time goes in v1:
time: 602 us; the launch traced here: 601 us
  waiting for transfers between devices  444 us (74%)
  matrix products  60.1 us (10%)
  blocking collectives  34.1 us (6%)
  local copies, waits for them, and re-layouts  25.1 us (4%)
  other arithmetic  18.5 us (3%)
  between operations  13.4 us (2%)
    all_gather x1, waiting for transfers between devices, per_device(): gate_hidden = add_rows(lax.all_gather(ffn_gate, 'fs', axis=0, tiled=True))  182 us
    all_gather x1, waiting for transfers between devices, per_device(): lax.all_gather(ffn_down, 'fs', axis=1, tiled=True)  104 us
    reduce_scatter x1, waiting for transfers between devices, per_device(): lax.psum_scatter(mixer_terms.astype(jnp.bfloat16), 'tp', scatter_dimensio...  43.9 us
    reduce_scatter x1, waiting for transfers between devices, per_device(): lax.psum_scatter(ffn_terms.astype(jnp.bfloat16), 'tp', scatter_dimension=...  42.8 us
    all_gather x1, waiting for transfers between devices, per_device(): lax.all_gather(out_weight, 'fs', axis=1, tiled=True)  28.8 us
    all_gather x1, waiting for transfers between devices, per_device(): resid_whole = lax.all_gather(resid_shard, 'tp', axis=1, tiled=True)  24.7 us
    dot_general x1, matrix products, per_device(): jnp.dot(hidden, lax.all_gather(ffn_down, 'fs', axis=1, tiled=True), prefe...  21 us
    all_gather x1, blocking collectives, per_device(): lax.all_gather(key_weight, 'fs', axis=0, tiled=True)  17.6 us
  transfers between devices with their start and end apart: 10, of which 9 were waited for; matrix products, arithmetic and copies ran while one was open for 10% of the time, Pallas kernels for 0%

profile of v1, /device:TPU:0, one launch (start us, length us, event | category | flops | bytes accessed | tf_op | source)
XLA Modules:
  0.0 601.4 jit_solution(747601244638357048)
XLA Ops:
  6.5 0.7 all-gather.8.cloned.1.call-update
  7.3 0.7 all-gather.10.cloned.1.call-update
  8.1 0.7 all-gather.12.cloned.1.call-update
  8.8 0.5 all-gather.14.cloned.1.call-update
  9.5 17.6 %all_gather.28 = bf16[2048,128]{1,0:T(8,128)(2,1)S(1)} all-gather(bf16[512,128]{1,0:T(8,128)(2,1)} %param.19), channel_id=1, replica_groups=mesh['rep'=2,'fs'=4,'tp'=4] {'fs'}, dimensions={0}, use_global_device_ids=true | all-gather | bytes 655360 | tf_op jit(solution)/shard_map/all_gather | solution.py:99
  27.0 16.6 %all_gather.30 = bf16[2048,128]{1,0:T(8,128)(2,1)S(1)} all-gather(bf16[512,128]{1,0:T(8,128)(2,1)} %param.18), channel_id=1, replica_groups=mesh['rep'=2,'fs'=4,'tp'=4] {'fs'}, dimensions={0}, use_global_device_ids=true | all-gather | bytes 655360 | tf_op jit(solution)/shard_map/all_gather | solution.py:98
  43.7 1.3 multiply_cosine_fusion
  45.0 1.2 all-gather.8.cloned.1.call-done
  46.1 3.2 fusion.25
  49.6 1.0 fusion.27
  50.6 1.9 copy-done
  52.5 1.5 fusion.36
  54.1 0.3 reshape.191
  54.4 3.9 fusion.35
  58.5 2.1 multiply_subtract_fusion
  60.6 1.0 maximum_multiply_fusion
  61.6 1.8 mul.286
  63.4 1.9 reshape_reshape.24
  65.3 10.4 %all-gather.10.cloned.1.call-done = bf16[2048,256]{1,0:T(8,128)(2,1)} async-done(((bf16[512,256]{1,0:T(8,128)(2,1)}), bf16[2048,256]{1,0:T(8,128)(2,1)}) %all-gather.10.cloned.1.call-update) | async-done | bytes 1048592 | tf_op jit(solution)/shard_map/all_gather | solution.py:100
  75.7 3.7 fusion.31
  79.4 0.5 reshape.193
  80.1 19.0 %while.15 = (s32[]{:T(128)}, f32[4,2,64,128]{3,2,1,0:T(8,128)S(1)}, f32[4,4,64,2,128]{4,2,3,1,0:T(8,128)S(1)}, f32[4,4,64,2,64]{2,0,1,4,3:T(4,128)}, f32[4,4,64,...) while((s32[]{:T(128)}, f32[4,2,64,128]{3,2,1,0:T(8,128)S(1)}, ...), condition=%wide.region_2.4_spmd.clone.clone.clone, body=%wide.region_1.3_spmd.clone.clone.clone.sunk | while | flops 176603408 | bytes 4415676 | solution.py:74
  80.3 2.1 constant_dynamic-slice_fusion.3
  82.8 0.5 convolution_multiply_fusion.2
  83.3 0.4 convolution_bitcast_fusion.3
  83.8 0.4 fusion.93
  84.3 0.7 convolution_add_fusion.2
  85.0 2.1 constant_dynamic-slice_fusion.3
  87.5 0.5 convolution_multiply_fusion.2
  88.0 0.4 convolution_bitcast_fusion.3
  88.5 0.4 fusion.93
  89.0 0.7 convolution_add_fusion.2
  89.7 2.1 constant_dynamic-slice_fusion.3
  92.2 0.5 convolution_multiply_fusion.2
  92.7 0.4 convolution_bitcast_fusion.3
  93.2 0.4 fusion.93
  93.7 0.7 convolution_add_fusion.2
  94.4 2.1 constant_dynamic-slice_fusion.3
  96.9 0.5 convolution_multiply_fusion.2
  97.4 0.4 convolution_bitcast_fusion.3
  97.9 0.4 fusion.93
  98.4 0.7 convolution_add_fusion.2
  99.1 0.4 bitcast_reduce_fusion
  99.7 0.7 multiply_reduce_fusion
  100.7 1.8 copy.35
  102.5 2.2 all-gather.12.cloned.1.call-done
  104.7 28.8 %all-gather.14.cloned.1.call-done = bf16[256,2048]{1,0:T(8,128)(2,1)} async-done(((bf16[256,512]{1,0:T(8,128)(2,1)}), bf16[256,2048]{1,0:T(8,128)(2,1)}) %all-gather.14.cloned.1.call-update) | async-done | bytes 1048592 | tf_op jit(solution)/shard_map/all_gather | solution.py:134
  133.5 1.2 mul.299
  134.7 2.0 sub.86
  136.8 9.9 %convolution_convert_fusion.1 = bf16[1024,2048]{1,0:T(8,128)(2,1)} fusion(bf16[256,2048]{1,0:T(8,128)(2,1)} %all-gather.14.cloned.1.call-done, bf16[1024,2048]{1,0:T(8,128)(2,1)} %copy-done, bf16[2048,256]{1,0:T(8,128)(2,1)} %all-gather.12.cloned.1.call-done, f32[128,8,2,128]{3,2,1,0:T(2,128)S(1)} %bitcast.115, f32[128,8,2,128]{3,2,1,0:T(2,128)} %bitcast.116, ...), kind=kOutput, calls=%fused_computation.45 | convolution fusion | flops 2152464384 | bytes 13632512 | tf_op jit(solution)/shard_map/dot_general | solution.py:132
  146.8 43.9 %reduce-scatter.3.cloned.1.call-done = bf16[1024,512]{1,0:T(8,128)(2,1)} async-done(((bf16[1024,2048]{1,0:T(8,128)(2,1)}), bf16[1024,512]{1,0:T(8,128)(2,1)}) %reduce-scatter.3.cloned.1.call-update) | async-done | bytes 1048592 | tf_op jit(solution)/shard_map/reduce_scatter | solution.py:137
  190.6 2.5 add_convert_fusion.1
  193.2 0.7 all-gather.18.cloned.1.call-update
  193.9 2.9 stack.8
  196.8 5.4 all-to-all-start
  202.2 0.7 all-gather.20.cloned.1.call-update
  203.0 24.7 %all-gather.16.cloned.1.call-done = bf16[1024,2048]{1,0:T(8,128)(2,1)} async-done(((bf16[1024,512]{1,0:T(8,128)(2,1)}), bf16[1024,2048]{1,0:T(8,128)(2,1)}) %all-gather.16.cloned.1.call-update) | async-done | bytes 4194320 | tf_op jit(solution)/shard_map/all_gather | solution.py:141
  227.7 3.1 fusion.28
  230.8 182.0 %all-gather.18.cloned.1.call-done = bf16[2048,1408]{1,0:T(8,128)(2,1)} async-done(((bf16[512,1408]{1,0:T(8,128)(2,1)}), bf16[2048,1408]{1,0:T(8,128)(2,1)}) %all-gather.18.cloned.1.call-update) | async-done | bytes 5767184 | tf_op jit(solution)/shard_map/all_gather | solution.py:147
  412.8 11.9 %fusion.33 = f32[1024,1408]{1,0:T(8,128)} fusion(bf16[2048,1408]{1,0:T(8,128)(2,1)} %all-gather.18.cloned.1.call-done, bf16[1024,2048]{1,0:T(8,128)(2,1)} %all-gather.16.cloned.1.call-done, f32[2048]{0:T(1024)S(1)} %copy-done.6, f32[1024]{0:T(1024)S(1)} %add_rsqrt_fusion), kind=kOutput, calls=%fused_computation.53 | convolution fusion | flops 5913968640 | bytes 15740928 | tf_op jit(solution)/shard_map/dot_general | solution.py:145
  424.7 103.9 %all-gather.20.cloned.1.call-done = bf16[1408,2048]{1,0:T(8,128)(2,1)} async-done(((bf16[1408,512]{1,0:T(8,128)(2,1)}), bf16[1408,2048]{1,0:T(8,128)(2,1)}) %all-gather.20.cloned.1.call-update) | async-done | bytes 5767184 | tf_op jit(solution)/shard_map/all_gather | solution.py:156
  528.6 21.0 %convolution_convert_fusion = bf16[1024,2048]{1,0:T(8,128)(2,1)} fusion(bf16[1408,2048]{1,0:T(8,128)(2,1)} %all-gather.20.cloned.1.call-done, f32[1024,1408]{1,0:T(8,128)} %fusion.33, bf16[2048,1408]{1,0:T(8,128)(2,1)} %bitcast.8, bf16[1024,2048]{1,0:T(8,128)(2,1)} %all-gather.16.cloned.1.call-done, f32[2048]{0:T(1024)S(1)} %copy-done.6, ...), kind=kOutput, calls=%fused_computation.44 | convolution fusion | flops 11830296576 | bytes 25702400 | tf_op jit(solution)/shard_map/dot_general | solution.py:154
  549.6 42.8 %reduce-scatter.5.cloned.1.call-done = bf16[1024,512]{1,0:T(8,128)(2,1)} async-done(((bf16[1024,2048]{1,0:T(8,128)(2,1)}), bf16[1024,512]{1,0:T(8,128)(2,1)}) %reduce-scatter.5.cloned.1.call-update) | async-done | bytes 1048592 | tf_op jit(solution)/shard_map/reduce_scatter | solution.py:159
  592.4 2.5 add_convert_fusion
  (66 shorter events, 3.6 us)
Async XLA Ops:
  6.5 42.8 %copy-start.5 = (f32[2048]{0:T(1024)S(1)}, f32[2048]{0:T(1024)}, u32[]{:S(2)}) copy-start(f32[2048]{0:T(1024)} %param.17) | copy-start | bytes 24580
  6.5 39.6 %all-gather.8.cloned.1.call-start = ((), (), s32[]{:S(2)}) async-start(), calls=%async_computation.3 | async-start | bytes 5242880 | tf_op jit(solution)/shard_map/all_gather | solution.py:94
  7.3 68.4 %all-gather.10.cloned.1.call-start = ((), (), s32[]{:S(2)}) async-start(), calls=%async_computation.4 | async-start | bytes 1310720 | tf_op jit(solution)/shard_map/all_gather | solution.py:100
  8.0 96.7 %all-gather.12.cloned.1.call-start = ((), (), s32[]{:S(2)}) async-start(), calls=%async_computation.5 | async-start | bytes 1310720 | tf_op jit(solution)/shard_map/all_gather | solution.py:101
  8.7 124.8 %all-gather.14.cloned.1.call-start = ((), (), s32[]{:S(2)}) async-start(), calls=%async_computation.6 | async-start | bytes 1310720 | tf_op jit(solution)/shard_map/all_gather | solution.py:134
  9.3 181.3 %reduce-scatter.3.cloned.1.call-start = ((), (), s32[]{:S(2)}) async-start(), calls=%async_computation.7 | async-start | bytes 5242880 | tf_op jit(solution)/shard_map/reduce_scatter | solution.py:137
  46.1 3.4 copy-start.1
  50.6 1.9 copy-start
  99.1 37.7 %copy-start.7 = (f32[2,128]{1,0:T(2,128)S(1)}, f32[2,128]{1,0:T(2,128)}, u32[]{:S(2)}) copy-start(f32[2,128]{1,0:T(2,128)} %param.23) | copy-start | bytes 3076
  136.8 53.9 %copy-start.3 = (bf16[1024,512]{1,0:T(8,128)(2,1)S(1)}, bf16[1024,512]{1,0:T(8,128)(2,1)}, u32[]{:S(2)}) copy-start(bf16[1024,512]{1,0:T(8,128)(2,1)} %param.16) | copy-start | bytes 3145732
  146.7 47.2 %copy-start.4 = (bf16[512,1408]{1,0:T(8,128)(2,1)S(1)}, bf16[512,1408]{1,0:T(8,128)(2,1)}, u32[]{:S(2)}) copy-start(bf16[512,1408]{1,0:T(8,128)(2,1)} %param.26) | copy-start | bytes 4325380
  146.7 81.0 %all-gather.16.cloned.1.call-start = ((), (), s32[]{:S(2)}) async-start(), calls=%async_computation.8 | async-start | bytes 5242880 | tf_op jit(solution)/shard_map/all_gather | solution.py:141
  193.1 219.7 %all-gather.18.cloned.1.call-start = ((), (), s32[]{:S(2)}) async-start(), calls=%async_computation.9 | async-start | bytes 7208960 | tf_op jit(solution)/shard_map/all_gather | solution.py:147
  196.8 216.1 %copy-start.6 = (f32[2048]{0:T(1024)S(1)}, f32[2048]{0:T(1024)}, u32[]{:S(2)}) copy-start(f32[2048]{0:T(1024)} %param.24) | copy-start | bytes 24580
  196.8 228.0 %all-to-all-start = ((bf16[4,512,1408]{2,1,0:T(8,128)(2,1)}), bf16[4,512,1408]{2,1,0:T(8,128)(2,1)}, u32[]{:S(2)}, u32[]{:S(2)}) async-start(bf16[4,512,1408]{2,1,0:T(8,128)(2,1)} %stack.8), calls=%async_computation.1 | async-start | bytes 11534336 | tf_op jit(solution)/shard_map/all_to_all | solution.py:150
  202.2 326.4 %all-gather.20.cloned.1.call-start = ((), (), s32[]{:S(2)}) async-start(), calls=%async_computation.10 | async-start | bytes 7208960 | tf_op jit(solution)/shard_map/all_gather | solution.py:156
  202.9 389.4 %reduce-scatter.5.cloned.1.call-start = ((), (), s32[]{:S(2)}) async-start(), calls=%async_computation.11 | async-start | bytes 5242880 | tf_op jit(solution)/shard_map/reduce_scatter | solution.py:159
  528.6 63.8 %copy-start.2 = (bf16[1024,512]{1,0:T(8,128)(2,1)S(1)}, bf16[1024,512]{1,0:T(8,128)(2,1)}, u32[]{:S(2)}) copy-start(bf16[1024,512]{1,0:T(8,128)(2,1)} %add_convert_fusion.1) | copy-start | bytes 3145732
Sparse Core Ops, SparseCore 0:
  8.9 37.1 all-gather.7
  47.7 27.9 all-gather.9
  77.3 27.3 all-gather.11
  106.1 27.3 all-gather.13
  146.8 43.7 reduce-scatter.2
  193.2 34.4 all-gather.15
  229.3 183.4 all-gather.17
  414.4 114.1 all-gather.19
  549.7 42.6 reduce-scatter.4
